TPU v7x, 32 devices: a whole 2x2x4 slice. The times are simulated.
32 devices in a mesh: sp: 4 (over z), fs: 4 (over y, x), tp: 2 (over core).
Axes of the slice: x: 2, y: 2, z: 4, core: 2. Of those that a mesh axis runs over, the one named last changes fastest.
Arguments:
- queries: bfloat16 [4, 1024, 512], P('fs', 'sp', 'tp'), may hold values from -60 to 60
- keys: bfloat16 [4, 1024, 256], P('fs', 'sp', 'tp'), may hold values from -4.5 to 4.5
- values: bfloat16 [4, 1024, 256], P('fs', 'sp', 'tp'), may hold values from -6 to 6
- forget_cache: float32 [4, 1024, 8], P('fs', 'sp', 'tp'), may hold values from -128 to 0, as said below
- fox_gain: float32 [512], P('tp'), may hold values from 0.1 to 1.9
- receptance: bfloat16 [4, 1024, 512], P('fs', 'sp', 'tp'), may hold values from -6 to 6
- lin_keys: bfloat16 [4, 1024, 512], P('fs', 'sp', 'tp'), may hold values from -6 to 6
- lin_values: bfloat16 [4, 1024, 512], P('fs', 'sp', 'tp'), may hold values from -6 to 6
- learn_logit: bfloat16 [4, 1024, 512], P('fs', 'sp', 'tp'), may hold values from -12 to 4
- decay_log: float32 [4, 1024, 512], P('fs', 'sp', 'tp'), may hold values from -16 to 0
- lin_gain: float32 [512], P('tp'), may hold values from 0.1 to 1.9
- out_fox_weight: bfloat16 [512, 2048], P('tp', 'fs'), may hold values from -0.1875 to 0.1875
- out_lin_weight: bfloat16 [512, 2048], P('tp', 'fs'), may hold values from -0.1875 to 0.1875
Outputs:
- mixed: bfloat16 [4, 1024, 2048], P('fs', ('sp', 'tp'))
Inputs may be any that keep to these rules, and one draw needn't show every extreme that they name: `forget_cache`: Non-increasing along the positions of each sequence and head.
All inputs are finite; a program needn't handle non-finite values.
Results may differ from a plain program's by a relative error of at most 0.017.
Values may be sent and summed in bfloat16 or wider, within the bound.
A program may use at most 64 MiB of HBM per device.

v0:
```python
import math
import jax
import jax.numpy as jnp
from jax import lax
from jax.sharding import PartitionSpec as P

HEAD = 64
SPAN = 64
HIGHEST = lax.Precision.HIGHEST
NORM_EPS = 1e-06


def carried_in(shard, axis, join, neutral):
    place = lax.axis_index(axis)
    gathered = jax.tree.map(
        lambda a, kind: lax.all_gather(a.astype(kind), axis), shard, (jnp.bfloat16, jnp.bfloat16)
    )
    state = jax.tree.map(lambda a, e: jnp.zeros_like(a) + jnp.asarray(e, a.dtype), shard, neutral)

    def one(lap, state):
        return join(
            state,
            jax.tree.map(
                lambda a, own: lax.dynamic_index_in_dim(a, lap, 0, False).astype(own.dtype),
                gathered,
                shard,
            ),
        )

    return lax.fori_loop(0, place, one, state)


def round_half(tensor):
    return lax.optimization_barrier(tensor.astype(jnp.bfloat16)).astype(jnp.float32)


def forget_attention(query_rows, key_rows, value_rows, forget_rows, fox_gain):
    row_count = query_rows.shape[0]
    head_count = query_rows.shape[1] // HEAD
    kv_count = key_rows.shape[1] // HEAD
    group_size = head_count // kv_count
    score_scale = HEAD ** (-0.5)
    own_first = lax.axis_index("sp") * row_count
    forget_all = lax.all_gather(forget_rows, "sp", axis=0, tiled=True)
    forget_own = forget_rows.reshape(row_count, kv_count, group_size)
    query_heads = query_rows.reshape(row_count, kv_count, group_size, HEAD)
    query_pos = own_first + jnp.arange(row_count, dtype=jnp.int32)
    start_state = (
        jnp.full((row_count, kv_count, group_size), -1e30, jnp.float32),
        jnp.zeros((row_count, kv_count, group_size), jnp.float32),
        jnp.zeros((row_count, kv_count, group_size, HEAD), jnp.float32),
    )
    key_piece = lax.all_gather(key_rows, "sp", axis=0, tiled=True)
    value_piece = lax.all_gather(value_rows, "sp", axis=0, tiled=True)
    piece_rows = key_piece.shape[0]
    block_rows = math.gcd(piece_rows, 512)

    def attend(state):

        def one_block(block_index, inner):
            running_max, totals, weighted = inner
            local_first = (block_index * block_rows).astype(jnp.int32)
            key_block = lax.dynamic_slice_in_dim(key_piece, local_first, block_rows, 0).reshape(
                block_rows, kv_count, HEAD
            )
            value_block = lax.dynamic_slice_in_dim(value_piece, local_first, block_rows, 0).reshape(
                block_rows, kv_count, HEAD
            )
            forget_block = lax.dynamic_slice_in_dim(forget_all, local_first, block_rows, 0).reshape(
                block_rows, kv_count, group_size
            )
            key_pos = local_first + jnp.arange(block_rows, dtype=jnp.int32)
            allowed = (key_pos[None, :] <= query_pos[:, None])[:, None, None, :]
            scores = jnp.einsum(
                "tkgd,skd->tkgs", query_heads, key_block, preferred_element_type=jnp.float32
            )
            scores = (
                scores * score_scale
                + forget_own[..., None]
                - jnp.transpose(forget_block, (1, 2, 0))[None]
            )
            scores = jnp.where(allowed, scores, -1e30)
            new_max = jnp.maximum(running_max, jnp.max(scores, axis=-1))
            rescale = jnp.exp(running_max - new_max)
            weights = jnp.where(allowed, jnp.exp(scores - new_max[..., None]), 0.0)
            totals = totals * rescale + jnp.sum(weights, axis=-1)
            update = jnp.einsum(
                "tkgs,skd->tkgd",
                weights.astype(jnp.bfloat16),
                value_block,
                preferred_element_type=jnp.float32,
            )
            weighted = weighted * rescale[..., None] + update
            return (new_max, totals, weighted)

        return lax.fori_loop(0, piece_rows // block_rows, one_block, state)

    def keep_state(running_state):
        return running_state

    running_max, totals, weighted = lax.cond(
        jnp.int32(0) < own_first + row_count, attend, keep_state, start_state
    )
    attended = (weighted / totals[..., None]).reshape(row_count, head_count, HEAD)
    normed = attended * lax.rsqrt(jnp.mean(attended * attended, axis=-1, keepdims=True) + NORM_EPS)
    return (
        (normed * fox_gain.reshape(head_count, HEAD))
        .reshape(row_count, head_count * HEAD)
        .astype(jnp.bfloat16)
    )


def product(left, right, form):
    return jnp.einsum(form, left, right, precision=HIGHEST)


def delta_attention(recept_rows, key_rows, value_rows, learn_rows, decay_rows, lin_gain):
    row_count = recept_rows.shape[0]
    head_count = recept_rows.shape[1] // HEAD
    span_count = row_count // SPAN

    def arrange(tensor):
        return jnp.transpose(
            tensor.astype(jnp.float32).reshape(span_count, SPAN, head_count, HEAD), (0, 2, 1, 3)
        )

    recept = arrange(recept_rows)
    key_float = arrange(key_rows)
    value_float = arrange(value_rows)
    learn_rate = jax.nn.sigmoid(arrange(learn_rows))
    unit_keys = key_float * lax.rsqrt(
        jnp.sum(key_float * key_float, axis=-1, keepdims=True) + NORM_EPS
    )
    log_decay = -jnp.exp(arrange(decay_rows))
    strict_lower = jnp.tril(jnp.ones((SPAN, SPAN), jnp.float32), -1)
    with_diagonal = jnp.tril(jnp.ones((SPAN, SPAN), jnp.float32))
    identity_head = jnp.broadcast_to(jnp.eye(HEAD, dtype=jnp.float32), (head_count, HEAD, HEAD))
    identity_span = jnp.broadcast_to(jnp.eye(SPAN, dtype=jnp.float32), (head_count, SPAN, SPAN))
    zero_state = jnp.zeros((head_count, HEAD, HEAD), jnp.float32)

    def one_span(state, inputs):
        recept_t, key_t, value_t, unit_t, rate_t, fall_t = inputs
        inclusive = jnp.cumsum(fall_t, axis=1)
        grown = jnp.exp(inclusive)
        shrunk = jnp.exp(-inclusive)
        erase_in = -unit_t * jnp.exp(inclusive - fall_t)
        read_in = recept_t * grown
        erase_out = unit_t * rate_t * shrunk
        write_out = key_t * shrunk
        padded_values = jnp.concatenate([value_t, jnp.zeros_like(value_t)], axis=-1)
        mix_erase = product(erase_in, erase_out, "hid,hjd->hij") * strict_lower
        mix_write = product(erase_in, write_out, "hid,hjd->hij") * strict_lower
        read_erase = product(read_in, erase_out, "hid,hjd->hij") * with_diagonal
        read_write = product(read_in, write_out, "hid,hjd->hij") * with_diagonal
        right_side = product(erase_in, state, "hid,hrd->hir") + product(
            mix_write, padded_values, "hij,hjr->hir"
        )
        erased = jax.scipy.linalg.solve_triangular(
            identity_span - mix_erase, right_side, lower=True, unit_diagonal=True
        )
        outputs = (
            product(read_in, state, "hid,hrd->hir")
            + product(read_erase, erased, "hij,hjr->hir")
            + product(read_write, padded_values, "hij,hjr->hir")
        )
        final_grow = grown[:, -1, :]
        state = (
            state * final_grow[:, None, :]
            + product(erased, erase_out * final_grow[:, None, :], "hlr,hld->hrd")
            + product(padded_values, write_out * final_grow[:, None, :], "hlr,hld->hrd")
        )
        return (state, outputs)

    start_state = jnp.concatenate([zero_state, identity_head], axis=1)
    final_state, outputs = lax.scan(
        one_span, start_state, (recept, key_float, value_float, unit_keys, learn_rate, log_decay)
    )
    local_read = outputs[..., :HEAD]
    carried_read = outputs[..., HEAD:]

    def chain(earlier, later):
        return (
            product(earlier[0], later[0], "hij,hjk->hik"),
            product(earlier[1], later[0], "hij,hjk->hik") + later[1],
        )

    entry_map, entry_state = carried_in(
        (final_state[:, HEAD:], final_state[:, :HEAD]), "sp", chain, (identity_head, zero_state)
    )
    readout = local_read + jnp.einsum(
        "hvk,nhtk->nhtv", entry_state, carried_read, precision=HIGHEST
    )
    readout = jnp.transpose(readout, (0, 2, 1, 3)).reshape(row_count, head_count, HEAD)
    centred = readout - jnp.mean(readout, axis=-1, keepdims=True)
    normed = centred * lax.rsqrt(jnp.mean(centred * centred, axis=-1, keepdims=True) + HEAD * 1e-05)
    return (
        (normed * lin_gain.reshape(head_count, HEAD))
        .reshape(row_count, head_count * HEAD)
        .astype(jnp.bfloat16)
    )


def shards(
    queries,
    keys,
    values,
    forget_cache,
    fox_gain,
    receptance,
    lin_keys,
    lin_values,
    learn_logit,
    decay_log,
    lin_gain,
    out_fox_weight,
    out_lin_weight,
):
    fox_out = forget_attention(queries[0], keys[0], values[0], forget_cache[0], fox_gain)
    lin_out = delta_attention(
        receptance[0], lin_keys[0], lin_values[0], learn_logit[0], decay_log[0], lin_gain
    )
    fox_weight, lin_weight = (
        lax.all_gather(out_fox_weight, "fs", axis=1, tiled=True),
        lax.all_gather(out_lin_weight, "fs", axis=1, tiled=True),
    )
    partial_value = jnp.dot(fox_out, fox_weight, preferred_element_type=jnp.float32)
    partial_value = partial_value + jnp.dot(lin_out, lin_weight, preferred_element_type=jnp.float32)
    summed = lax.psum_scatter(
        round_half(partial_value).astype(jnp.bfloat16), "tp", scatter_dimension=0, tiled=True
    )
    return summed[None]


def solution(mesh):
    return jax.shard_map(
        shards,
        mesh=mesh,
        in_specs=(
            P("fs", "sp", "tp"),
            P("fs", "sp", "tp"),
            P("fs", "sp", "tp"),
            P("fs", "sp", "tp"),
            P("tp"),
            P("fs", "sp", "tp"),
            P("fs", "sp", "tp"),
            P("fs", "sp", "tp"),
            P("fs", "sp", "tp"),
            P("fs", "sp", "tp"),
            P("tp"),
            P("tp", "fs"),
            P("tp", "fs"),
        ),
        out_specs=P("fs", ("sp", "tp"), None),
        check_vma=False,
    )
```

profile of v0, /device:TPU:0, one launch (start us, length us, event | category | flops | bytes accessed | tf_op | source)
XLA Modules:
  0.0 230.0 jit_solution(1138776864522754009)
XLA Ops:
  8.1 1.2 reshape.164
  10.2 1.1 reshape.163
  13.0 106.6 %while.46 = (s32[]{:T(128)}, f32[4,128,64]{1,2,0:T(8,128)S(1)}, f32[4,4,64,128]{3,2,1,0:T(8,128)}, f32[4,4,64,64]{3,1,2,0:T(4,128)}, f32[4,4,64,64]{3,1,2,0:T(4,...) while((s32[]{:T(128)}, f32[4,128,64]{1,2,0:T(8,128)S(1)}, ...), condition=%wide.region_10.11_spmd.clone.clone, body=%wide.region_8.10_spmd.clone.clone.sunk | while | flops 253308992 | bytes 5993869 | solution.py:175
  15.6 19.7 %custom-call.11 = f32[4,1,64,64]{2,3,1,0:T(8,128)S(1)} custom-call(f32[4,1,64,64]{3,2,1,0:T(8,128)S(1)} %fusion.172), custom_call_target="InvertDiagBlocksLowerTriangular" | custom-call | tf_op jit(solution)/shard_map/while/body/eval_jaxpr/jit(_solve_triangular)/vmap()/triangular_solve | solution.py:158
  42.2 19.7 %custom-call.11 = f32[4,1,64,64]{2,3,1,0:T(8,128)S(1)} custom-call(f32[4,1,64,64]{3,2,1,0:T(8,128)S(1)} %fusion.172), custom_call_target="InvertDiagBlocksLowerTriangular" | custom-call | tf_op jit(solution)/shard_map/while/body/eval_jaxpr/jit(_solve_triangular)/vmap()/triangular_solve | solution.py:158
  68.9 19.7 %custom-call.11 = f32[4,1,64,64]{2,3,1,0:T(8,128)S(1)} custom-call(f32[4,1,64,64]{3,2,1,0:T(8,128)S(1)} %fusion.172), custom_call_target="InvertDiagBlocksLowerTriangular" | custom-call | tf_op jit(solution)/shard_map/while/body/eval_jaxpr/jit(_solve_triangular)/vmap()/triangular_solve | solution.py:158
  95.5 19.7 %custom-call.11 = f32[4,1,64,64]{2,3,1,0:T(8,128)S(1)} custom-call(f32[4,1,64,64]{3,2,1,0:T(8,128)S(1)} %fusion.172), custom_call_target="InvertDiagBlocksLowerTriangular" | custom-call | tf_op jit(solution)/shard_map/while/body/eval_jaxpr/jit(_solve_triangular)/vmap()/triangular_solve | solution.py:158
  119.7 15.7 %all-gather.3 = bf16[16,64,64]{2,1,0:T(8,128)(2,1)S(1)} all-gather(bf16[4,64,64]{2,1,0:T(8,128)(2,1)S(1)} %get-tuple-element.533), channel_id=5, replica_groups=mesh['sp'=4,'fs'=4,'tp'=2] {'sp'}, dimensions={0}, use_global_device_ids=true | all-gather | bytes 163840 | tf_op jit(solution)/shard_map/all_gather | solution.py:16
  135.4 14.6 %all-gather.4 = bf16[16,64,64]{2,1,0:T(8,128)(2,1)S(1)} all-gather(bf16[4,64,64]{2,1,0:T(8,128)(2,1)S(1)} %get-tuple-element.532), channel_id=6, replica_groups=mesh['sp'=4,'fs'=4,'tp'=2] {'sp'}, dimensions={0}, use_global_device_ids=true | all-gather | bytes 163840 | tf_op jit(solution)/shard_map/all_gather | solution.py:16
  151.4 1.7 fusion.65
  156.0 13.2 %all-gather.1 = f32[1,1024,4]{1,2,0:T(4,128)S(1)} all-gather(f32[1,256,4]{1,2,0:T(4,128)S(1)} %copy-done.10), channel_id=3, replica_groups=mesh['sp'=4,'fs'=4,'tp'=2] {'sp'}, dimensions={1}, use_global_device_ids=true | all-gather | bytes 20480 | tf_op jit(solution)/shard_map/all_gather | solution.py:44
  169.2 14.5 %all-gather = bf16[1,1024,128]{1,2,0:T(8,128)(2,1)S(1)} all-gather(bf16[1,256,128]{1,2,0:T(8,128)(2,1)S(1)} %copy.55), channel_id=2, replica_groups=mesh['sp'=4,'fs'=4,'tp'=2] {'sp'}, dimensions={1}, use_global_device_ids=true | all-gather | bytes 327680 | tf_op jit(solution)/shard_map/all_gather | solution.py:53
  183.7 14.0 %all-gather.2 = bf16[1,1024,128]{1,2,0:T(8,128)(2,1)S(1)} all-gather(bf16[1,256,128]{1,2,0:T(8,128)(2,1)S(1)} %copy.56), channel_id=4, replica_groups=mesh['sp'=4,'fs'=4,'tp'=2] {'sp'}, dimensions={1}, use_global_device_ids=true | all-gather | bytes 327680 | tf_op jit(solution)/shard_map/all_gather | solution.py:54
  197.7 10.5 %conditional.1 = (f32[256,2,2]{0,2,1:T(2,128)}, f32[256,2,2,64]{0,3,2,1:T(8,128)}) conditional(s32[]{:T(128)} %convert_element_type.58, () %tuple.38, (s32[]{:T(128)}, s32[256]{0:T(256)S(1)}, bf16[1,256,256]{2,1,0:T(8,128)(2,1)S(1)}, bf16[1024,128]{0,1:T(8,128)(2,1)S(1)}, f32[1,256,4]{1,2,0:T(4,128)S(1)}, /*index=5*/f32[1024,4]{0,1:T(4,128)S(1)}, ...), branch_computations={%region_0.0_spmd, %region_1.6_spmd} | conditional | flops 140318464 | bytes 8662403 | solution.py:101
  198.5 9.7 %while.44 = (s32[]{:T(128)}, f32[256,2,2]{0,2,1:T(2,128)S(1)}, f32[256,2,2]{0,2,1:T(2,128)}, f32[256,2,2,64]{0,3,2,1:T(8,128)}, s32[256]{0:T(256)S(1)}, /*index=...) while((s32[]{:T(128)}, f32[256,2,2]{0,2,1:T(2,128)S(1)}, ...), condition=%wide.wide.region_5.5_spmd.clone, body=%wide.wide.region_2.4_spmd.clone.sunk | while | flops 140318208 | bytes 8373459 | solution.py:96
  198.7 1.6 fusion.181
  201.4 1.2 fusion.185
  202.8 1.6 fusion.181
  204.8 1.3 fusion.184
  206.1 2.1 fusion.185
  208.2 1.1 multiply_reduce_fusion.2
  209.5 1.7 fusion.67
  211.2 2.7 %fusion.54 = bf16[256,2048]{1,0:T(8,128)(2,1)} fusion(f32[256,2048]{1,0:T(8,128)S(1)} %fusion.67, bf16[256,2048]{1,0:T(8,128)(2,1)} %all-gather.10.cloned.1.call-done, f32[256,256]{1,0:T(8,128)S(1)} %copy-done.1, f32[256,256]{1,0:T(8,128)S(1)} %reshape.160, f32[256,256]{1,0:T(8,128)S(1)} %copy-done.2, f32[256]{0:T(256)S(1)} %copy-done.13), kind=kOutput, calls=%fused_computation.87 | convolution fusion | flops 269746176 | bytes 4981760 | tf_op jit(solution)/shard_map/dot_general | solution.py:227
  213.9 9.5 %reduce-scatter.2.cloned.1.call-done = bf16[128,2048]{1,0:T(8,128)(2,1)} async-done(((bf16[256,2048]{1,0:T(8,128)(2,1)}), bf16[128,2048]{1,0:T(8,128)(2,1)}) %reduce-scatter.2.cloned.1.call-update) | async-done | bytes 524304 | tf_op jit(solution)/shard_map/reduce_scatter | solution.py:228
  (191 shorter events, 38.5 us)
Async XLA Ops:
  6.5 3.6 %copy-start.4 = (bf16[1,256,256]{2,1,0:T(8,128)(2,1)S(1)}, bf16[1,256,256]{2,1,0:T(8,128)(2,1)}, u32[]{:S(2)}) copy-start(bf16[1,256,256]{2,1,0:T(8,128)(2,1)} %param.29) | copy-start | bytes 393220
  6.5 202.9 %all-gather.8.cloned.1.call-start = ((), (), s32[]{:S(2)}) async-start(), calls=%async_computation.1 | async-start | bytes 1310720 | tf_op jit(solution)/shard_map/all_gather | solution.py:223
  7.3 4.0 %copy-start.3 = (f32[1,256,256]{2,1,0:T(8,128)S(1)}, f32[1,256,256]{2,1,0:T(8,128)}, u32[]{:S(2)}) copy-start(f32[1,256,256]{2,1,0:T(8,128)} %param.30) | copy-start | bytes 786436
  7.3 203.9 %all-gather.10.cloned.1.call-start = ((), (), s32[]{:S(2)}) async-start(), calls=%async_computation.2 | async-start | bytes 1310720 | tf_op jit(solution)/shard_map/all_gather | solution.py:224
  8.0 215.4 %reduce-scatter.2.cloned.1.call-start = ((), (), s32[]{:S(2)}) async-start(), calls=%async_computation.3 | async-start | bytes 1572864 | tf_op jit(solution)/shard_map/reduce_scatter | solution.py:228
  9.6 2.7 %copy-start.5 = (bf16[1,256,256]{2,1,0:T(8,128)(2,1)S(1)}, bf16[1,256,256]{2,1,0:T(8,128)(2,1)}, u32[]{:S(2)}) copy-start(bf16[1,256,256]{2,1,0:T(8,128)(2,1)} %param.28) | copy-start | bytes 393220
  9.7 2.9 %copy-start.6 = (bf16[1,256,256]{2,1,0:T(8,128)(2,1)S(1)}, bf16[1,256,256]{2,1,0:T(8,128)(2,1)}, u32[]{:S(2)}) copy-start(bf16[1,256,256]{2,1,0:T(8,128)(2,1)} %param.26) | copy-start | bytes 393220
  150.0 1.0 copy-start
  153.1 2.7 %copy-start.8 = (bf16[1,256,128]{2,1,0:T(8,128)(2,1)S(1)}, bf16[1,256,128]{2,1,0:T(8,128)(2,1)}, u32[]{:S(2)}) copy-start(bf16[1,256,128]{2,1,0:T(8,128)(2,1)} %param.22) | copy-start | bytes 196612
  153.1 2.8 %copy-start.9 = (bf16[1,256,128]{2,1,0:T(8,128)(2,1)S(1)}, bf16[1,256,128]{2,1,0:T(8,128)(2,1)}, u32[]{:S(2)}) copy-start(bf16[1,256,128]{2,1,0:T(8,128)(2,1)} %param.23) | copy-start | bytes 196612
  153.1 2.9 %copy-start.10 = (f32[1,256,4]{1,2,0:T(4,128)S(1)}, f32[1,256,4]{1,2,0:T(4,128)}, u32[]{:S(2)}) copy-start(f32[1,256,4]{1,2,0:T(4,128)} %param.24) | copy-start | bytes 12292
  153.4 44.3 %copy-start.7 = (bf16[1,256,256]{2,1,0:T(8,128)(2,1)S(1)}, bf16[1,256,256]{2,1,0:T(8,128)(2,1)}, u32[]{:S(2)}) copy-start(bf16[1,256,256]{2,1,0:T(8,128)(2,1)} %param.21) | copy-start | bytes 393220
  197.7 11.6 %copy-start.12 = (f32[256]{0:T(256)S(1)}, f32[256]{0:T(256)}, u32[]{:S(2)}) copy-start(f32[256]{0:T(256)} %param.25) | copy-start | bytes 3076
  197.7 0.8 copy-start.11
  208.2 3.0 %copy-start.1 = (f32[256,256]{1,0:T(8,128)S(1)}, f32[256,256]{1,0:T(8,128)}, u32[]{:S(2)}) copy-start(f32[256,256]{1,0:T(8,128)} %copy.73) | copy-start | bytes 786436
  208.2 3.0 %copy-start.2 = (f32[256,256]{1,0:T(8,128)S(1)}, f32[256,256]{1,0:T(8,128)}, u32[]{:S(2)}) copy-start(f32[256,256]{1,0:T(8,128)} %copy.72) | copy-start | bytes 786436
  208.2 3.0 %copy-start.13 = (f32[256]{0:T(256)S(1)}, f32[256]{0:T(256)}, u32[]{:S(2)}) copy-start(f32[256]{0:T(256)} %param.31) | copy-start | bytes 3076
Sparse Core Ops, SparseCore 0:
  9.2 29.8 all-gather.7
  40.9 27.0 all-gather.9
  214.0 9.3 reduce-scatter.1
where the time goes:
time: 231 us; the launch traced here: 230 us
  other arithmetic  85.3 us (37%)
  blocking collectives  71.9 us (31%)
  matrix products  30.9 us (13%)
  local copies, waits for them, and re-layouts  16.6 us (7%)
  between operations  13.5 us (6%)
  waiting for transfers between devices  11 us (5%)
    another operation x12, other arithmetic, one_span(): jax.scipy.linalg.solve_triangular(identity_span - mix_erase, right_side,...  79 us
    all_gather x2, blocking collectives, carried_in(): lax.all_gather(a.astype(kind), axis)  30.2 us
    dot_general x44, matrix products, product(): return jnp.einsum(form, left, right, precision=HIGHEST)  16.7 us
    all_gather x1, blocking collectives, forget_attention(): key_piece = lax.all_gather(key_rows, 'sp', axis=0, tiled=True)  14.5 us
    all_gather x1, blocking collectives, forget_attention(): value_piece = lax.all_gather(value_rows, 'sp', axis=0, tiled=True)  14 us
    all_gather x1, blocking collectives, forget_attention(): forget_all = lax.all_gather(forget_rows, 'sp', axis=0, tiled=True)  13.2 us
    reduce_scatter x1, waiting for transfers between devices, shards(): lax.psum_scatter(round_half(partial_value).astype(jnp.bfloat16), 'tp', sc...  9.53 us
    dynamic_slice x20, local copies, waits for them, and re-layouts, delta_attention(): lax.scan(one_span, start_state, (recept, key_float, value_float, unit_key...  7.59 us
  transfers between devices with their start and end apart: 3, of which 1 were waited for; matrix products, arithmetic and copies ran while one was open for 56% of the time, Pallas kernels for 0%

commit v1 on v0

--- a/solution.py
+++ b/solution.py
@@ -3,11 +3,20 @@
 import jax.numpy as jnp
 from jax import lax
 from jax.sharding import PartitionSpec as P
+from jax.lax import all_gather
 
 HEAD = 64
 SPAN = 64
 HIGHEST = lax.Precision.HIGHEST
 NORM_EPS = 1e-06
+
+
+def define_the_patches(point, my_tile):
+    return jnp.split(
+        all_gather(jnp.concatenate([point, my_tile], 1), "sp", tiled=True, axis=0),
+        [point.shape[1]],
+        1,
+    )
 
 
 def carried_in(shard, axis, join, neutral):
@@ -41,7 +50,6 @@
     group_size = head_count // kv_count
     score_scale = HEAD ** (-0.5)
     own_first = lax.axis_index("sp") * row_count
-    forget_all = lax.all_gather(forget_rows, "sp", axis=0, tiled=True)
     forget_own = forget_rows.reshape(row_count, kv_count, group_size)
     query_heads = query_rows.reshape(row_count, kv_count, group_size, HEAD)
     query_pos = own_first + jnp.arange(row_count, dtype=jnp.int32)
@@ -50,7 +58,7 @@
         jnp.zeros((row_count, kv_count, group_size), jnp.float32),
         jnp.zeros((row_count, kv_count, group_size, HEAD), jnp.float32),
     )
-    key_piece = lax.all_gather(key_rows, "sp", axis=0, tiled=True)
+    forget_all, key_piece = define_the_patches(forget_rows, key_rows)
     value_piece = lax.all_gather(value_rows, "sp", axis=0, tiled=True)
     piece_rows = key_piece.shape[0]
     block_rows = math.gcd(piece_rows, 512)

time: 231 us -> 224 us (0.970)
  blocking collectives: 71.9 us -> 59.8 us
  other arithmetic: 85.3 us -> 87.9 us
    all_gather x2 -> x1, blocking collectives: 27.7 us -> 15.5 us  [define_the_patches(): all_gather(jnp.concatenate([point, my_tile], 1), 'sp', tiled=True, axis=0)]
  transfers between devices with their start and end apart: 3 -> 3, of which waited for: 1 -> 1; matrix products, arithmetic and copies ran while one was open for 56% -> 60% of each run, Pallas kernels for 0% -> 0%
where the time goes in v1:
time: 224 us; the launch traced here: 223 us
  other arithmetic  87.9 us (39%)
  blocking collectives  59.8 us (27%)
  matrix products  30.9 us (14%)
  local copies, waits for them, and re-layouts  18.5 us (8%)
  between operations  13.5 us (6%)
  waiting for transfers between devices  11.6 us (5%)
    another operation x12, other arithmetic, one_span(): jax.scipy.linalg.solve_triangular(identity_span - mix_erase, right_side,...  79 us
    all_gather x2, blocking collectives, carried_in(): lax.all_gather(a.astype(kind), axis)  30.2 us
    dot_general x44, matrix products, product(): return jnp.einsum(form, left, right, precision=HIGHEST)  16.7 us
    all_gather x1, blocking collectives, define_the_patches(): all_gather(jnp.concatenate([point, my_tile], 1), 'sp', tiled=True, axis=0)  15.5 us
    all_gather x1, blocking collectives, forget_attention(): value_piece = lax.all_gather(value_rows, 'sp', axis=0, tiled=True)  14.1 us
    reduce_scatter x1, waiting for transfers between devices, shards(): lax.psum_scatter(round_half(partial_value).astype(jnp.bfloat16), 'tp', sc...  10.2 us
    dynamic_slice x20, local copies, waits for them, and re-layouts, delta_attention(): lax.scan(one_span, start_state, (recept, key_float, value_float, unit_key...  7.59 us
  transfers between devices with their start and end apart: 3, of which 1 were waited for; matrix products, arithmetic and copies ran while one was open for 60% of the time, Pallas kernels for 0%

profile of v1, /device:TPU:0, one launch (start us, length us, event | category | flops | bytes accessed | tf_op | source)
XLA Modules:
  0.0 223.0 jit_solution(17254553038363002301)
XLA Ops:
  8.1 1.2 reshape.167
  10.2 1.0 reshape.166
  11.3 1.0 neg.24
  13.0 106.6 %while.46 = (s32[]{:T(128)}, f32[4,128,64]{1,2,0:T(8,128)S(1)}, f32[4,4,64,128]{3,2,1,0:T(8,128)}, f32[4,4,64,64]{3,1,2,0:T(4,128)}, f32[4,4,64,64]{3,1,2,0:T(4,...) while((s32[]{:T(128)}, f32[4,128,64]{1,2,0:T(8,128)S(1)}, ...), condition=%wide.region_10.11_spmd.clone.clone, body=%wide.region_8.10_spmd.clone.clone.sunk | while | flops 253308992 | bytes 5993869 | solution.py:183
  15.6 19.7 %custom-call.11 = f32[4,1,64,64]{2,3,1,0:T(8,128)S(1)} custom-call(f32[4,1,64,64]{3,2,1,0:T(8,128)S(1)} %fusion.172), custom_call_target="InvertDiagBlocksLowerTriangular" | custom-call | tf_op jit(solution)/shard_map/while/body/eval_jaxpr/jit(_solve_triangular)/vmap()/triangular_solve | solution.py:166
  42.2 19.7 %custom-call.11 = f32[4,1,64,64]{2,3,1,0:T(8,128)S(1)} custom-call(f32[4,1,64,64]{3,2,1,0:T(8,128)S(1)} %fusion.172), custom_call_target="InvertDiagBlocksLowerTriangular" | custom-call | tf_op jit(solution)/shard_map/while/body/eval_jaxpr/jit(_solve_triangular)/vmap()/triangular_solve | solution.py:166
  68.9 19.7 %custom-call.11 = f32[4,1,64,64]{2,3,1,0:T(8,128)S(1)} custom-call(f32[4,1,64,64]{3,2,1,0:T(8,128)S(1)} %fusion.172), custom_call_target="InvertDiagBlocksLowerTriangular" | custom-call | tf_op jit(solution)/shard_map/while/body/eval_jaxpr/jit(_solve_triangular)/vmap()/triangular_solve | solution.py:166
  95.5 19.7 %custom-call.11 = f32[4,1,64,64]{2,3,1,0:T(8,128)S(1)} custom-call(f32[4,1,64,64]{3,2,1,0:T(8,128)S(1)} %fusion.172), custom_call_target="InvertDiagBlocksLowerTriangular" | custom-call | tf_op jit(solution)/shard_map/while/body/eval_jaxpr/jit(_solve_triangular)/vmap()/triangular_solve | solution.py:166
  119.7 15.7 %all-gather.1 = bf16[16,64,64]{2,1,0:T(8,128)(2,1)S(1)} all-gather(bf16[4,64,64]{2,1,0:T(8,128)(2,1)S(1)} %get-tuple-element.530), channel_id=3, replica_groups=mesh['sp'=4,'fs'=4,'tp'=2] {'sp'}, dimensions={0}, use_global_device_ids=true | all-gather | bytes 163840 | tf_op jit(solution)/shard_map/all_gather | solution.py:25
  135.4 14.6 %all-gather.2 = bf16[16,64,64]{2,1,0:T(8,128)(2,1)S(1)} all-gather(bf16[4,64,64]{2,1,0:T(8,128)(2,1)S(1)} %get-tuple-element.529), channel_id=4, replica_groups=mesh['sp'=4,'fs'=4,'tp'=2] {'sp'}, dimensions={0}, use_global_device_ids=true | all-gather | bytes 163840 | tf_op jit(solution)/shard_map/all_gather | solution.py:25
  151.3 1.7 fusion.65
  155.3 14.1 %all-gather = bf16[1,1024,128]{1,2,0:T(8,128)(2,1)S(1)} all-gather(bf16[1,256,128]{1,2,0:T(8,128)(2,1)S(1)} %copy.56), channel_id=2, replica_groups=mesh['sp'=4,'fs'=4,'tp'=2] {'sp'}, dimensions={1}, use_global_device_ids=true | all-gather | bytes 327680 | tf_op jit(solution)/shard_map/all_gather | solution.py:62
  169.4 15.5 %all_gather.24 = f32[1024,132]{0,1:T(8,128)S(1)} all-gather(f32[256,132]{0,1:T(8,128)S(1)} %pad_maximum_fusion), channel_id=1, replica_groups=mesh['sp'=4,'fs'=4,'tp'=2] {'sp'}, dimensions={0}, use_global_device_ids=true | all-gather | bytes 675840 | tf_op jit(solution)/shard_map/all_gather | solution.py:16
  184.9 15.0 %conditional.1 = (f32[256,2,2]{0,2,1:T(2,128)}, f32[256,2,2,64]{0,3,2,1:T(8,128)}) conditional(s32[]{:T(128)} %convert_element_type.64, () %tuple.38, (f32[1024,132]{0,1:T(8,128)S(1)}, s32[]{:T(128)}, s32[256]{0:T(256)S(1)}, bf16[1,256,256]{2,1,0:T(8,128)(2,1)S(1)}, f32[1,256,4]{1,2,0:T(4,128)S(1)}, /*index=5*/bf16[1024,128]{0,1:T(8,128)(2,1)S(1)}) %tuple.143), branch_computations={%region_0.0_spmd, %region_1.6_spmd} | conditional | flops 140318464 | bytes 9219459 | solution.py:109
  187.5 12.4 %while.44 = (s32[]{:T(128)}, f32[256,2,2]{0,2,1:T(2,128)S(1)}, f32[256,2,2]{0,2,1:T(2,128)}, f32[256,2,2,64]{0,3,2,1:T(8,128)}, s32[256]{0:T(256)}, /*index=5*/b...) while((s32[]{:T(128)}, f32[256,2,2]{0,2,1:T(2,128)S(1)}, ...), condition=%wide.wide.region_5.5_spmd.clone, body=%wide.wide.region_2.4_spmd.clone.sunk | while | flops 140318208 | bytes 8373459 | solution.py:104
  189.1 1.6 fusion.181
  191.8 1.2 fusion.185
  194.5 1.6 fusion.181
  196.5 1.3 fusion.184
  197.8 2.1 fusion.185
  200.0 1.0 multiply_reduce_fusion.2
  201.9 1.7 fusion.67
  203.6 2.7 %fusion.54 = bf16[256,2048]{1,0:T(8,128)(2,1)} fusion(f32[256,2048]{1,0:T(8,128)S(1)} %fusion.67, bf16[256,2048]{1,0:T(8,128)(2,1)} %all-gather.8.cloned.1.call-done, f32[256,256]{1,0:T(8,128)S(1)} %copy.73, f32[256,256]{1,0:T(8,128)S(1)} %reshape.162, f32[256,256]{1,0:T(8,128)S(1)} %copy-done.1, f32[256]{0:T(256)S(1)} %copy-done.11), kind=kOutput, calls=%fused_computation.87 | convolution fusion | flops 269746176 | bytes 4981760 | tf_op jit(solution)/shard_map/dot_general | solution.py:235
  206.3 10.2 %reduce-scatter.2.cloned.1.call-done = bf16[128,2048]{1,0:T(8,128)(2,1)} async-done(((bf16[256,2048]{1,0:T(8,128)(2,1)}), bf16[128,2048]{1,0:T(8,128)(2,1)}) %reduce-scatter.2.cloned.1.call-update) | async-done | bytes 524304 | tf_op jit(solution)/shard_map/reduce_scatter | solution.py:236
  (190 shorter events, 42.0 us)
Async XLA Ops:
  6.5 3.6 %copy-start.3 = (bf16[1,256,256]{2,1,0:T(8,128)(2,1)S(1)}, bf16[1,256,256]{2,1,0:T(8,128)(2,1)}, u32[]{:S(2)}) copy-start(bf16[1,256,256]{2,1,0:T(8,128)(2,1)} %param.29) | copy-start | bytes 393220
  6.5 195.3 %all-gather.6.cloned.1.call-start = ((), (), s32[]{:S(2)}) async-start(), calls=%async_computation.1 | async-start | bytes 1310720 | tf_op jit(solution)/shard_map/all_gather | solution.py:231
  7.3 4.0 %copy-start.2 = (f32[1,256,256]{2,1,0:T(8,128)S(1)}, f32[1,256,256]{2,1,0:T(8,128)}, u32[]{:S(2)}) copy-start(f32[1,256,256]{2,1,0:T(8,128)} %param.30) | copy-start | bytes 786436
  7.3 196.3 %all-gather.8.cloned.1.call-start = ((), (), s32[]{:S(2)}) async-start(), calls=%async_computation.2 | async-start | bytes 1310720 | tf_op jit(solution)/shard_map/all_gather | solution.py:232
  8.0 208.5 %reduce-scatter.2.cloned.1.call-start = ((), (), s32[]{:S(2)}) async-start(), calls=%async_computation.3 | async-start | bytes 1572864 | tf_op jit(solution)/shard_map/reduce_scatter | solution.py:236
  9.6 2.7 %copy-start.4 = (bf16[1,256,256]{2,1,0:T(8,128)(2,1)S(1)}, bf16[1,256,256]{2,1,0:T(8,128)(2,1)}, u32[]{:S(2)}) copy-start(bf16[1,256,256]{2,1,0:T(8,128)(2,1)} %param.28) | copy-start | bytes 393220
  9.7 2.9 %copy-start.5 = (bf16[1,256,256]{2,1,0:T(8,128)(2,1)S(1)}, bf16[1,256,256]{2,1,0:T(8,128)(2,1)}, u32[]{:S(2)}) copy-start(bf16[1,256,256]{2,1,0:T(8,128)(2,1)} %param.26) | copy-start | bytes 393220
  149.9 1.0 copy-start
  153.1 1.9 copy-start.7
  153.1 2.0 copy-start.8
  153.4 16.0 %copy-start.9 = (f32[1,256,4]{1,2,0:T(4,128)S(1)}, f32[1,256,4]{1,2,0:T(4,128)}, u32[]{:S(2)}) copy-start(f32[1,256,4]{1,2,0:T(4,128)} %param.24) | copy-start | bytes 12292
  153.5 31.5 %copy-start.6 = (bf16[1,256,256]{2,1,0:T(8,128)(2,1)S(1)}, bf16[1,256,256]{2,1,0:T(8,128)(2,1)}, u32[]{:S(2)}) copy-start(bf16[1,256,256]{2,1,0:T(8,128)(2,1)} %param.21) | copy-start | bytes 393220
  184.9 2.6 %copy-start.10 = (f32[1,256,4]{1,2,0:T(4,128)}, f32[1,256,4]{1,2,0:T(4,128)S(1)}, u32[]{:S(2)}) copy-start(f32[1,256,4]{1,2,0:T(4,128)S(1)} %get-tuple-element.786) | copy-start | bytes 12292 | tf_op jit(solution)/shard_map/cond
  200.0 3.6 %copy-start.1 = (f32[256,256]{1,0:T(8,128)S(1)}, f32[256,256]{1,0:T(8,128)}, u32[]{:S(2)}) copy-start(f32[256,256]{1,0:T(8,128)} %copy.72) | copy-start | bytes 786436
  200.0 3.6 %copy-start.11 = (f32[256]{0:T(256)S(1)}, f32[256]{0:T(256)}, u32[]{:S(2)}) copy-start(f32[256]{0:T(256)} %param.31) | copy-start | bytes 3076
Sparse Core Ops, SparseCore 0:
  9.2 29.8 all-gather.5
  40.9 27.0 all-gather.7
  206.4 10.0 reduce-scatter.1
